TPU v7x, 32 devices: a whole 2x2x4 slice. The times are simulated.
32 devices in a mesh: ep: 8 (over z, x), tp: 4 (over y, core).
Axes of the slice: x: 2, y: 2, z: 4, core: 2. Of those that a mesh axis runs over, the one named last changes fastest.
Arguments:
- queries: bfloat16 [2048, 1024], P('ep', 'tp'), may hold values from -5 to 5
- keys: bfloat16 [2048, 1024], P('ep', 'tp'), may hold values from -5 to 5
- values: bfloat16 [2048, 1024], P('ep', 'tp'), may hold values from -6 to 6
- gate_totals: float32 [2048, 8], P('ep', 'tp'), as said below
- out_proj: bfloat16 [1024, 2048], P('tp'), may hold values from -0.75 to 0.75
- moe_input: bfloat16 [3072, 2048], P('ep'), may hold values from -600 to 600
- norm_gain: float32 [2048], replicated, may hold values from 0.1 to 1.9
- routes: int32 [3072, 2], P('ep'), may hold values from 0 to 7, all different within a row; in each aligned block of 384 rows (0 to 383, 384 to 767, ...) at most 100 rows name the same one
- route_logits: float32 [3072, 2], P('ep'), may hold values from -6 to 6
- expert_gate: bfloat16 [8, 2048, 3072], P('ep', None, 'tp'), may hold values from -0.125 to 0.125
- expert_up: bfloat16 [8, 2048, 3072], P('ep', None, 'tp'), may hold values from -0.125 to 0.125
- expert_down: bfloat16 [8, 3072, 2048], P('ep', 'tp'), may hold values from -0.109375 to 0.109375
Outputs:
- mixed: bfloat16 [2048, 2048], P('ep', 'tp')
- routed: bfloat16 [3072, 2048], P('ep', 'tp')
Inputs may be any that keep to these rules, and one draw needn't show every extreme that they name: `gate_totals`: along the positions, each head's values never increase. `routes`: A token names 2 different experts. Among the 384 tokens of one index of ep no expert is named more than 100 times, and in some of these blocks one expert is named exactly 100 times.
All inputs are finite; a program needn't handle non-finite values.
Results may differ from a plain program's by a relative error of at most 0.01.
Values may be sent and summed in bfloat16 or wider, within the bound.
A program may use at most 128 MiB of HBM per device.

v0:
```python
import math

import jax
import jax.numpy as jnp
from jax import lax
from jax.sharding import PartitionSpec as P

epsilon = 1e-06
far_below = -1e30


def expert_hidden(rows, gate_part, up_part):
    gate_rows = jnp.einsum("scd,df->scf", rows, gate_part, preferred_element_type=jnp.float32)
    up_rows = jnp.einsum("scd,df->scf", rows, up_part, preferred_element_type=jnp.float32)
    return (jax.nn.silu(gate_rows) * up_rows).astype(jnp.bfloat16)


def body(
    queries,
    keys,
    values,
    gate_totals,
    out_proj,
    moe_input,
    norm_gain,
    routes,
    route_logits,
    expert_gate,
    expert_up,
    expert_down,
):
    tok_rows, local_heads = gate_totals.shape
    head_size = queries.shape[1] // local_heads
    width = out_proj.shape[1]
    scale = 1.0 / math.sqrt(head_size)
    first_row = lax.axis_index("ep") * tok_rows
    query_pos = first_row + lax.iota(jnp.int32, tok_rows)
    query_heads = queries.reshape(tok_rows, local_heads, head_size)
    query_totals = jnp.transpose(gate_totals)
    all_totals = lax.all_gather(gate_totals, "ep", axis=0, tiled=True)

    def update(carry, block_keys, block_values, block_start):
        run_max, running_total, run_acc = carry
        count = block_keys.shape[0]
        key_heads = block_keys.reshape(count, local_heads, head_size)
        value_heads = block_values.reshape(count, local_heads, head_size)
        key_totals = jnp.transpose(lax.dynamic_slice_in_dim(all_totals, block_start, count, 0))
        scores = (
            jnp.einsum("qhd,khd->hqk", query_heads, key_heads, preferred_element_type=jnp.float32)
            * scale
        )
        scores = scores + query_totals[:, :, None] - key_totals[:, None, :]
        key_pos = block_start + lax.iota(jnp.int32, count)
        causal = key_pos[None, :] <= query_pos[:, None]
        scores = jnp.where(causal[None, :, :], scores, -jnp.inf)
        new_max = jnp.maximum(run_max, jnp.max(scores, axis=2))
        weights = jnp.exp(scores - new_max[:, :, None])
        shrink = jnp.exp(run_max - new_max)
        new_sum = running_total * shrink + jnp.sum(weights, axis=2)
        summed = jnp.einsum(
            "hqk,khd->hqd",
            weights.astype(jnp.bfloat16),
            value_heads,
            preferred_element_type=jnp.float32,
        )
        return (new_max, new_sum, run_acc * shrink[:, :, None] + summed)

    initial = (
        jnp.full((local_heads, tok_rows), far_below, jnp.float32),
        jnp.zeros((local_heads, tok_rows), jnp.float32),
        jnp.zeros((local_heads, tok_rows, head_size), jnp.float32),
    )
    piece_keys = lax.all_gather(keys, "ep", axis=0, tiled=True)
    piece_values = lax.all_gather(values, "ep", axis=0, tiled=True)
    count = piece_keys.shape[0]
    span = math.gcd(count, 512)

    def one_span(index, state):
        offset = index * span
        block_keys = lax.dynamic_slice_in_dim(piece_keys, offset, span, 0)
        block_values = lax.dynamic_slice_in_dim(piece_values, offset, span, 0)
        return update(state, block_keys, block_values, offset)

    run_max, running_total, run_acc = lax.fori_loop(0, count // span, one_span, initial)
    head_mix = (run_acc / running_total[:, :, None]).astype(jnp.bfloat16)
    head_weights = out_proj.reshape(local_heads, head_size, width)
    attn_term = jnp.einsum(
        "hqd,hdn->qn", head_mix, head_weights, preferred_element_type=jnp.float32
    )
    tok_b, width_b = moe_input.shape
    top = routes.shape[1]
    ep_count = lax.axis_size("ep")
    tp_count = lax.axis_size("tp")
    capacity = tp_count * (tok_b * top // (tp_count * ep_count) + 1)
    moe_float = moe_input.astype(jnp.float32)
    normed = (
        moe_float
        * lax.rsqrt(jnp.mean(moe_float * moe_float, axis=1, keepdims=True) + epsilon)
        * norm_gain
    ).astype(jnp.bfloat16)
    flat_routes = routes.reshape(tok_b * top)
    expert_ids = lax.iota(jnp.int32, ep_count)
    indicator_matrix = (flat_routes[:, None] == expert_ids[None, :]).astype(jnp.int32)
    earlier = jnp.cumsum(indicator_matrix, axis=0) - indicator_matrix
    rank = jnp.sum(earlier * indicator_matrix, axis=1)
    slot_of = flat_routes * capacity + rank
    token_of = lax.iota(jnp.int32, tok_b * top) // top
    source = jnp.full((ep_count * capacity,), tok_b, jnp.int32).at[slot_of].set(token_of)
    padded = jnp.concatenate([normed, jnp.zeros((1, width_b), jnp.bfloat16)], axis=0)
    outgoing = jnp.take(padded, source, axis=0).reshape(ep_count, capacity, width_b)
    gate_part = expert_gate[0]
    up_part = expert_up[0]
    down_part = expert_down[0]
    arrived = lax.all_to_all(outgoing, "ep", split_axis=0, concat_axis=0, tiled=True)
    hidden = expert_hidden(arrived, gate_part, up_part)
    unit_term = jnp.einsum(
        "scf,fd->scd", hidden, down_part, preferred_element_type=jnp.float32
    ).reshape(ep_count * capacity, width_b)
    attn_sum, unit_sum = (
        lax.psum_scatter(
            attn_term.astype(jnp.bfloat16), "tp", scatter_dimension=1, tiled=True
        ).astype(jnp.float32),
        lax.psum_scatter(
            unit_term.astype(jnp.bfloat16), "tp", scatter_dimension=1, tiled=True
        ).astype(jnp.float32),
    )
    mixed = attn_sum.astype(jnp.bfloat16)
    expert_rows = unit_sum.astype(jnp.bfloat16).reshape(ep_count, capacity, unit_sum.shape[1])
    returned = lax.all_to_all(expert_rows, "ep", split_axis=0, concat_axis=0, tiled=True)
    picked = jnp.take(
        returned.reshape(ep_count * capacity, returned.shape[2]), slot_of, axis=0
    ).reshape(tok_b, top, returned.shape[2])
    route_weights = jax.nn.sigmoid(route_logits - route_logits[:, ::-1])
    routed = jnp.sum(picked.astype(jnp.float32) * route_weights[:, :, None], axis=1).astype(
        jnp.bfloat16
    )
    return (mixed, routed)


def solution(mesh):
    return jax.shard_map(
        body,
        mesh=mesh,
        in_specs=(
            P("ep", "tp"),
            P("ep", "tp"),
            P("ep", "tp"),
            P("ep", "tp"),
            P("tp", None),
            P("ep", None),
            P(),
            P("ep", None),
            P("ep", None),
            P("ep", None, "tp"),
            P("ep", None, "tp"),
            P("ep", "tp", None),
        ),
        out_specs=(P("ep", "tp"), P("ep", "tp")),
        check_vma=False,
    )
```

profile of v0, /device:TPU:0, one launch (start us, length us, event | category | flops | bytes accessed | tf_op | source)
XLA Modules:
  0.0 264.0 jit_solution(9373132992948759001)
XLA Ops:
  13.2 3.4 %scatter_custom_fusion = s32[800]{0:T(1024)S(1)} fusion(s32[768]{0:T(1024)S(1)} %fusion.30, s32[768]{0:T(1024)S(1)} %add_select_fusion, s32[]{:T(128)} %constant.117.clone.1), kind=kCustom, calls=%fused_computation.68 | custom fusion | bytes 3204 | tf_op jit(solution)/shard_map/scatter | solution.py:108
  21.5 10.3 %gather_fusion = bf16[800,2048]{1,0:T(8,128)(2,1)} fusion(bf16[385,2048]{1,0:T(8,128)(2,1)} %concatenate.3, s32[1024]{0:T(1024)S(1)} %pad_clamp_fusion.1), kind=kCustom, calls=%fused_computation | custom fusion | bytes 6556800 | tf_op jit(solution)/shard_map/jit(_take)/gather | solution.py:110
  31.8 4.5 %gather.13 = bf16[8,100,2048]{2,1,0:T(8,128)(2,1)} reshape(bf16[800,2048]{1,0:T(8,128)(2,1)} %gather_fusion) | data formatting | bytes 6553600 | tf_op jit(solution)/shard_map/jit(_take)/gather | solution.py:110
  36.4 4.1 %broadcast_select_fusion.1 = bf16[8,100,2048]{2,1,0:T(8,128)(2,1)} fusion(bf16[8,100,2048]{2,1,0:T(8,128)(2,1)} %gather.13, pred[8,100]{1,0:T(8,128)(4,1)S(1)} %broadcast_in_dim.95), kind=kLoop, calls=%fused_computation.29 | loop fusion | flops 1638400 | bytes 6554400 | tf_op jit(solution)/shard_map/jit(_take)/select_n | solution.py:110
  40.5 7.4 %all-to-all-start = ((bf16[8,100,2048]{2,1,0:T(8,128)(2,1)}), bf16[8,100,2048]{2,1,0:T(8,128)(2,1)}, u32[]{:S(2)}, u32[]{:S(2)}) async-start(bf16[8,100,2048]{2,1,0:T(8,128)(2,1)} %broadcast_select_fusion.1), calls=%async_computation.1 | async-start | bytes 6815744 | tf_op jit(solution)/shard_map/all_to_all | solution.py:114
  50.0 107.2 %all_gather.10 = f32[2048,2]{0,1:T(2,128)} all-gather(f32[256,2]{0,1:T(2,128)} %param.17), channel_id=1, replica_groups=mesh['ep'=8,'tp'=4] {'ep'}, dimensions={0}, use_global_device_ids=true | all-gather | bytes 18432 | tf_op jit(solution)/shard_map/all_gather | solution.py:40
  157.1 5.9 %fusion.16 = f32[8,100,768]{2,1,0:T(8,128)S(1)} fusion(bf16[8,100,2048]{2,1,0:T(8,128)(2,1)} %all-to-all-done, bf16[1,2048,768]{2,1,0:T(8,128)(2,1)} %param.24), kind=kOutput, calls=%fused_computation.34 | convolution fusion | flops 2516582400 | bytes 8880128 | tf_op jit(solution)/shard_map/scd,df->scf/dot_general | solution.py:14
  163.1 6.1 %multiply_convert_fusion = bf16[8,100,768]{2,1,0:T(8,128)(2,1)} fusion(f32[8,100,768]{2,1,0:T(8,128)S(1)} %fusion.16, bf16[8,100,2048]{2,1,0:T(8,128)(2,1)} %all-to-all-done, bf16[1,2048,768]{2,1,0:T(8,128)(2,1)S(1)} %copy-done.8), kind=kOutput, calls=%fused_computation.40 | convolution fusion | flops 2520268800 | bytes 10108928 | tf_op jit(solution)/shard_map/scd,df->scf/dot_general | solution.py:13
  169.2 2.3 dot_general.29
  171.5 5.4 %convolution_convert_fusion = bf16[800,2048]{1,0:T(8,128)(2,1)} fusion(bf16[800,768]{1,0:T(8,128)(2,1)} %dot_general.29, bf16[1,768,2048]{2,1,0:T(8,128)(2,1)S(1)} %copy-done), kind=kOutput, calls=%fused_computation.28 | convolution fusion | flops 2518220800 | bytes 7651328 | tf_op jit(solution)/shard_map/scf,fd->scd/dot_general | solution.py:116
  177.0 31.4 %while.18 = (s32[]{:T(128)}, f32[2,256]{1,0:T(2,128)S(1)}, f32[2,256]{1,0:T(2,128)S(1)}, f32[2,256,128]{2,1,0:T(8,128)}, bf16[2048,256]{0,1:T(8,128)(2,1)}, /*in...) while((s32[]{:T(128)}, f32[2,256]{1,0:T(2,128)S(1)}, ...), condition=%wide.region_3.4_spmd.clone, body=%wide.region_0.3_spmd.clone.sunk | while | flops 136908032 | bytes 5689551 | solution.py:84
  178.9 2.1 fusion.53
  182.7 2.4 convolution_add_fusion.2
  190.5 2.4 convolution_add_fusion.2
  198.3 2.3 convolution_add_fusion.2
  206.0 2.3 convolution_add_fusion.2
  208.4 2.8 %fusion.20 = bf16[256,2048]{1,0:T(8,128)(2,1)} fusion(bf16[2,128,2048]{2,1,0:T(8,128)(2,1)} %bitcast.59, f32[2,256,128]{2,1,0:T(8,128)} %get-tuple-element.172, f32[2,256]{1,0:T(2,128)S(1)} %get-tuple-element.173), kind=kOutput, calls=%fused_computation.39 | convolution fusion | flops 269090816 | bytes 2361344 | tf_op jit(solution)/shard_map/hqd,hdn->qn/dot_general | solution.py:87
  212.7 2.1 reshape.157
  214.8 5.5 %all-to-all-start.1 = ((bf16[8,100,512]{2,1,0:T(8,128)(2,1)}), bf16[8,100,512]{2,1,0:T(8,128)(2,1)}, u32[]{:S(2)}, u32[]{:S(2)}) async-start(bf16[8,100,512]{2,1,0:T(8,128)(2,1)} %reshape.157), calls=%async_computation.3 | async-start | bytes 1703936 | tf_op jit(solution)/shard_map/all_to_all | solution.py:129
  221.2 20.8 %all-to-all-done.1 = bf16[8,100,512]{2,1,0:T(8,128)(2,1)} async-done(((bf16[8,100,512]{2,1,0:T(8,128)(2,1)}), bf16[8,100,512]{2,1,0:T(8,128)(2,1)}, u32[]{:S(2)}, u32[]{:S(2)}) %all-to-all-start.1) | async-done | bytes 819232 | tf_op jit(solution)/shard_map/all_to_all | solution.py:129
  242.0 2.1 reshape.158
  244.1 4.6 %gather_fusion.1 = bf16[768,512]{1,0:T(8,128)(2,1)} fusion(bf16[800,512]{1,0:T(8,128)(2,1)} %reshape.158, s32[1024]{0:T(1024)S(1)} %pad_clamp_fusion), kind=kCustom, calls=%fused_computation.1 | custom fusion | bytes 1575936 | tf_op jit(solution)/shard_map/jit(_take)/gather | solution.py:130
  248.7 2.9 %gather.15 = bf16[384,2,512]{2,1,0:T(2,128)(2,1)} reshape(bf16[768,512]{1,0:T(8,128)(2,1)} %gather_fusion.1) | data formatting | bytes 1572864 | tf_op jit(solution)/shard_map/jit(_take)/gather | solution.py:130
  251.6 5.0 %multiply_reduce_fusion = bf16[384,512]{1,0:T(8,128)(2,1)} fusion(bf16[384,2,512]{2,1,0:T(2,128)(2,1)} %gather.15, pred[384,2]{1,0:T(8,128)(4,1)S(1)} %copy.44, f32[384,2]{1,0:T(8,128)S(1)} %copy.46), kind=kLoop, calls=%fused_computation.41 | loop fusion | flops 1376256 | bytes 1183488 | tf_op jit(solution)/shard_map/reduce_sum | solution.py:134
  (108 shorter events, 34.1 us)
Async XLA Ops:
  8.0 163.5 %copy-start = (bf16[1,768,2048]{2,1,0:T(8,128)(2,1)S(1)}, bf16[1,768,2048]{2,1,0:T(8,128)(2,1)}, u32[]{:S(2)}) copy-start(bf16[1,768,2048]{2,1,0:T(8,128)(2,1)} %param.25) | copy-start | bytes 9437188
  12.6 0.6 copy-start.5
  40.5 7.5 %copy-start.1 = (bf16[256,256]{1,0:T(8,128)(2,1)S(1)}, bf16[256,256]{1,0:T(8,128)(2,1)}, u32[]{:S(2)}) copy-start(bf16[256,256]{1,0:T(8,128)(2,1)} %param.15) | copy-start | bytes 393220
  40.5 8.3 %copy-start.2 = (bf16[256,256]{1,0:T(8,128)(2,1)S(1)}, bf16[256,256]{1,0:T(8,128)(2,1)}, u32[]{:S(2)}) copy-start(bf16[256,256]{1,0:T(8,128)(2,1)} %param.16) | copy-start | bytes 393220
  40.5 9.2 %copy-start.3 = (bf16[256,256]{1,0:T(8,128)(2,1)S(1)}, bf16[256,256]{1,0:T(8,128)(2,1)}, u32[]{:S(2)}) copy-start(bf16[256,256]{1,0:T(8,128)(2,1)} %param.14) | copy-start | bytes 393220
  40.5 116.6 %all-to-all-start = ((bf16[8,100,2048]{2,1,0:T(8,128)(2,1)}), bf16[8,100,2048]{2,1,0:T(8,128)(2,1)}, u32[]{:S(2)}, u32[]{:S(2)}) async-start(bf16[8,100,2048]{2,1,0:T(8,128)(2,1)} %broadcast_select_fusion.1), calls=%async_computation.1 | async-start | bytes 6815744 | tf_op jit(solution)/shard_map/all_to_all | solution.py:114
  47.9 129.0 %all-gather.3.cloned.1.call-start = ((), (), s32[]{:S(2)}) async-start(), calls=%async_computation.4 | async-start | bytes 1179648 | tf_op jit(solution)/shard_map/all_gather | solution.py:73
  48.8 128.2 %all-gather.5.cloned.1.call-start = ((), (), s32[]{:S(2)}) async-start(), calls=%async_computation.5 | async-start | bytes 1179648 | tf_op jit(solution)/shard_map/all_gather | solution.py:74
  49.6 163.1 %reduce-scatter.5.cloned.1.call-start = ((), (), s32[]{:S(2)}) async-start(), calls=%async_computation.7 | async-start | bytes 4096000 | tf_op jit(solution)/shard_map/reduce_scatter | solution.py:123
  157.1 5.9 %copy-start.8 = (bf16[1,2048,768]{2,1,0:T(8,128)(2,1)S(1)}, bf16[1,2048,768]{2,1,0:T(8,128)(2,1)}, u32[]{:S(2)}) copy-start(bf16[1,2048,768]{2,1,0:T(8,128)(2,1)} %param.23) | copy-start | bytes 9437188
  176.9 79.7 %reduce-scatter.3.cloned.1.call-start = ((), (), s32[]{:S(2)}) async-start(), calls=%async_computation.6 | async-start | bytes 1310720 | tf_op jit(solution)/shard_map/reduce_scatter | solution.py:120
  208.4 12.2 %copy-start.4 = (s32[384,2]{0,1:T(2,128)S(1)}, s32[384,2]{0,1:T(2,128)}, u32[]{:S(2)}) copy-start(s32[384,2]{0,1:T(2,128)} %param.21) | copy-start | bytes 9220
  208.4 12.5 %copy-start.7 = (f32[384,2]{0,1:T(2,128)S(1)}, f32[384,2]{0,1:T(2,128)}, u32[]{:S(2)}) copy-start(f32[384,2]{0,1:T(2,128)} %param.22) | copy-start | bytes 9220
  208.4 12.8 %copy-start.6 = (s32[768]{0:T(1024)S(1)}, s32[768]{0:T(1024)}, u32[]{:S(2)}) copy-start(s32[768]{0:T(1024)} %copy-done.5) | copy-start | bytes 9220
  214.8 27.1 %all-to-all-start.1 = ((bf16[8,100,512]{2,1,0:T(8,128)(2,1)}), bf16[8,100,512]{2,1,0:T(8,128)(2,1)}, u32[]{:S(2)}, u32[]{:S(2)}) async-start(bf16[8,100,512]{2,1,0:T(8,128)(2,1)} %reshape.157), calls=%async_computation.3 | async-start | bytes 1703936 | tf_op jit(solution)/shard_map/all_to_all | solution.py:129
Sparse Core Ops, SparseCore 0:
  51.4 74.8 all-gather.2
  128.3 39.7 all-gather.4
Sparse Core Ops, SparseCore 1:
  177.0 35.7 reduce-scatter.4
  215.7 24.7 reduce-scatter.2
where the time goes:
time: 265 us; the launch traced here: 264 us
  blocking collectives  107 us (40%)
  local copies, waits for them, and re-layouts  45.4 us (17%)
  matrix products  38.1 us (14%)
  waiting for transfers between devices  22.4 us (8%)
  other arithmetic  21.9 us (8%)
  between operations  15.8 us (6%)
  starting transfers between devices  13.1 us (5%)
    all_gather x1, blocking collectives, body(): all_totals = lax.all_gather(gate_totals, 'ep', axis=0, tiled=True)  107 us
    all_to_all x1, waiting for transfers between devices, body(): lax.all_to_all(expert_rows, 'ep', split_axis=0, concat_axis=0, tiled=True)  20.8 us
    gather x2, local copies, waits for them, and re-layouts, body(): jnp.take(padded, source, axis=0).reshape(ep_count, capacity, width_b)  14.8 us
    dot_general x4, matrix products, update(): jnp.einsum('hqk,khd->hqd', weights.astype(jnp.bfloat16), value_heads, pre...  9.44 us
    dot_general x4, matrix products, update(): jnp.einsum('qhd,khd->hqk', query_heads, key_heads, preferred_element_type...  8.38 us
    gather x2, local copies, waits for them, and re-layouts, body(): jnp.take(returned.reshape(ep_count * capacity, returned.shape[2]), slot_o...  7.47 us
    all_to_all x1, starting transfers between devices, body(): lax.all_to_all(outgoing, 'ep', split_axis=0, concat_axis=0, tiled=True)  7.41 us
    dot_general x1, matrix products, expert_hidden(): jnp.einsum('scd,df->scf', rows, gate_part, preferred_element_type=jnp.flo...  6.15 us
  transfers between devices with their start and end apart: 6, of which 2 were waited for; matrix products, arithmetic and copies ran while one was open for 28% of the time, Pallas kernels for 0%

commit v1 on v0

v1 whole, which is shorter than its diff:
```python
import functools
import math

import jax
import jax.numpy as jnp
from jax import lax
from jax.experimental import pallas as pl
from jax.experimental.pallas import tpu as pltpu
from jax.sharding import PartitionSpec as P

epsilon = 1e-06
far_below = -1e30
f32 = jnp.float32
bf16 = jnp.bfloat16


def attention_kernel(heads, span, spans, start_ref, q_ref, k_ref, v_ref, qt_ref, kt_ref, w_ref, out_ref, mix_ref):
    rows = q_ref.shape[0]
    hd = q_ref.shape[1] // heads
    scale = 1.0 / math.sqrt(hd)
    first = start_ref[0]
    step_rows = min(rows, 128)
    for h in range(heads):
        cols = slice(h * hd, (h + 1) * hd)
        for r in range(rows // step_rows):
            rsl = slice(r * step_rows, (r + 1) * step_rows)
            q = q_ref[rsl, cols]
            qt = qt_ref[rsl, h : h + 1]
            row_pos = first + r * step_rows + lax.broadcasted_iota(jnp.int32, (step_rows, 1), 0)

            def one(i, carry, q=q, qt=qt, row_pos=row_pos, cols=cols, h=h):
                top, total, acc = carry
                at = pl.multiple_of(i * span, span)
                k = k_ref[pl.ds(at, span), cols]
                v = v_ref[pl.ds(at, span), cols]
                s = lax.dot_general(q, k, (((1,), (1,)), ((), ())), preferred_element_type=f32) * scale
                s = s + qt - kt_ref[h : h + 1, pl.ds(at, span)]
                pos = at + lax.broadcasted_iota(jnp.int32, (1, span), 1)
                s = jnp.where(pos <= row_pos, s, far_below)
                new = jnp.maximum(top, jnp.max(s, axis=1, keepdims=True))
                w = jnp.where(pos <= row_pos, jnp.exp(s - new), 0.0)
                shrink = jnp.exp(top - new)
                total = total * shrink + jnp.sum(w, axis=1, keepdims=True)
                acc = acc * shrink + jnp.dot(w.astype(bf16), v, preferred_element_type=f32)
                return new, total, acc

            init = (
                jnp.full((step_rows, 1), far_below, f32),
                jnp.zeros((step_rows, 1), f32),
                jnp.zeros((step_rows, hd), f32),
            )
            _, total, acc = lax.fori_loop(0, spans, one, init)
            mix_ref[rsl, cols] = (acc / total).astype(bf16)
    out_ref[...] = jnp.dot(mix_ref[...], w_ref[...], preferred_element_type=f32).astype(bf16)


def attention(first_row, queries, keys, values, q_totals, k_totals, out_proj, heads):
    rows, width = queries.shape
    count = keys.shape[0]
    span = math.gcd(count, 1024)
    vm = pl.BlockSpec(memory_space=pltpu.VMEM)
    return pl.pallas_call(
        functools.partial(attention_kernel, heads, span, count // span),
        out_shape=jax.ShapeDtypeStruct((rows, out_proj.shape[1]), bf16),
        in_specs=[pl.BlockSpec(memory_space=pltpu.SMEM)] + [vm] * 6,
        out_specs=vm,
        scratch_shapes=[pltpu.VMEM((rows, width), bf16)],
        compiler_params=pltpu.CompilerParams(vmem_limit_bytes=40 << 20),
        cost_estimate=pl.CostEstimate(
            flops=4_000_000_000, bytes_accessed=4 * count * width, transcendentals=rows * count * heads
        ),
        name="attention",
    )(first_row[None], queries, keys, values, q_totals, k_totals, out_proj)


def three_terms(x):
    hi = lax.reduce_precision(x, 8, 7)
    rest = x - hi
    mid = lax.reduce_precision(rest, 8, 7)
    return jnp.concatenate([hi, mid, rest - mid], axis=1).astype(bf16)


def body(
    queries,
    keys,
    values,
    gate_totals,
    out_proj,
    moe_input,
    norm_gain,
    routes,
    route_logits,
    expert_gate,
    expert_up,
    expert_down,
):
    tok_rows, local_heads = gate_totals.shape
    width = out_proj.shape[1]
    part_width = keys.shape[1]
    tok_b, width_b = moe_input.shape
    top = routes.shape[1]
    ep_count = lax.axis_size("ep")
    tp_count = lax.axis_size("tp")
    capacity = tp_count * (tok_b * top // (tp_count * ep_count) + 1)
    slots = ep_count * capacity
    quarter = width_b // tp_count
    my_tp = lax.axis_index("tp")

    flat = jnp.transpose(routes).reshape(1, top * tok_b)
    chosen = (lax.broadcasted_iota(jnp.int32, (ep_count, 1), 0) == flat).astype(bf16)
    line = lax.iota(jnp.int32, top * tok_b)
    order = (line % tok_b) * top + line // tok_b
    before = (order[:, None] < order[None, :]).astype(bf16)
    counts = jnp.dot(chosen, before, preferred_element_type=f32)
    rank = jnp.sum(counts * chosen.astype(f32), axis=0).astype(jnp.int32)
    slot_of = (flat[0] * capacity + rank).reshape(top, tok_b)
    slot_ids = lax.iota(jnp.int32, slots)
    hits = [slot_of[k][None, :] == slot_ids[:, None] for k in range(top)]
    pick = functools.reduce(jnp.logical_or, hits).astype(bf16)

    moe_float = moe_input.astype(f32)
    mean = jnp.mean(moe_float * moe_float, axis=1, keepdims=True)
    mine = lax.dynamic_slice_in_dim(moe_input, my_tp * quarter, quarter, 1).astype(f32)
    gain = lax.dynamic_slice_in_dim(norm_gain, my_tp * quarter, quarter, 0)
    normed = (mine * lax.rsqrt(mean + epsilon) * gain).astype(bf16)
    outgoing = jnp.dot(pick, normed, preferred_element_type=f32).astype(bf16)
    arrived = lax.all_to_all(
        outgoing.reshape(ep_count, capacity, quarter), "ep", split_axis=0, concat_axis=0, tiled=True
    ).reshape(slots, quarter)

    shared = jnp.concatenate(
        [keys, values, jnp.pad(three_terms(gate_totals), ((0, 0), (0, 128 - 3 * local_heads)))], axis=1
    )
    everyone = lax.all_gather(shared, "ep", axis=0, tiled=True)
    terms = everyone[:, 2 * part_width : 2 * part_width + 3 * local_heads].astype(f32)
    all_totals = (
        terms[:, :local_heads] + terms[:, local_heads : 2 * local_heads] + terms[:, 2 * local_heads :]
    )
    attn_term = attention(
        lax.axis_index("ep") * tok_rows,
        queries,
        everyone[:, :part_width],
        everyone[:, part_width : 2 * part_width],
        gate_totals,
        jnp.transpose(all_totals),
        out_proj,
        local_heads,
    )
    mixed = lax.psum_scatter(attn_term, "tp", scatter_dimension=1, tiled=True)

    rows = lax.all_gather(arrived, "tp", axis=0, tiled=True).reshape(tp_count, slots, quarter)
    gate_w = expert_gate[0].reshape(tp_count, quarter, -1)
    up_w = expert_up[0].reshape(tp_count, quarter, -1)
    gate_rows = sum(jnp.dot(rows[i], gate_w[i], preferred_element_type=f32) for i in range(tp_count))
    up_rows = sum(jnp.dot(rows[i], up_w[i], preferred_element_type=f32) for i in range(tp_count))
    hidden = (jax.nn.silu(gate_rows) * up_rows).astype(bf16)
    unit_term = jnp.dot(hidden, expert_down[0], preferred_element_type=f32).astype(bf16)
    expert_rows = lax.psum_scatter(unit_term, "tp", scatter_dimension=1, tiled=True)
    returned = lax.all_to_all(
        expert_rows.reshape(ep_count, capacity, quarter), "ep", split_axis=0, concat_axis=0, tiled=True
    ).reshape(slots, quarter)

    route_weights = jax.nn.sigmoid(route_logits - route_logits[:, ::-1])
    place = sum(
        jnp.where(slot_of[k][:, None] == slot_ids[None, :], route_weights[:, k : k + 1], 0.0)
        for k in range(top)
    )
    place_hi = lax.reduce_precision(place, 8, 7)
    place_lo = (place - place_hi).astype(bf16)
    routed = (
        jnp.dot(place_hi.astype(bf16), returned, preferred_element_type=f32)
        + jnp.dot(place_lo, returned, preferred_element_type=f32)
    ).astype(bf16)
    return (mixed, routed)


def solution(mesh):
    return jax.shard_map(
        body,
        mesh=mesh,
        in_specs=(
            P("ep", "tp"),
            P("ep", "tp"),
            P("ep", "tp"),
            P("ep", "tp"),
            P("tp", None),
            P("ep", None),
            P(),
            P("ep", None),
            P("ep", None),
            P("ep", None, "tp"),
            P("ep", None, "tp"),
            P("ep", "tp", None),
        ),
        out_specs=(P("ep", "tp"), P("ep", "tp")),
        check_vma=False,
    )
```

time: 265 us -> 217 us (0.82)
  blocking collectives: 107 us -> 29.7 us
  waiting for transfers between devices: 22.4 us -> 96.9 us
  local copies, waits for them, and re-layouts: 45.4 us -> 23.4 us
  other arithmetic: 21.9 us -> 3.39 us
  starting transfers between devices: 13.1 us -> 5.86 us
  Pallas kernels: 0 us -> 4.98 us
    all_gather x1 -> x0, blocking collectives: 107 us -> none  [body(): all_totals = lax.all_gather(gate_totals, 'ep', axis=0, tiled=True)]
    all_gather x2, waiting for transfers between devices: 0.04 us -> 54.7 us  [the longest x1 28 us: body(): everyone = lax.all_gather(shared, 'ep', axis=0, tiled=True)]
    all_to_all x0 -> x1, blocking collectives: none -> 29.7 us  [body(): lax.all_to_all(outgoing.reshape(ep_count, capacity, quarter), 'ep', split...]
    gather x4 -> x0, local copies, waits for them, and re-layouts: 22.3 us -> none  [the longest x2 14.8 us: body(): jnp.take(padded, source, axis=0).reshape(ep_count, capacity, width_b)]
    reduce_scatter x2, waiting for transfers between devices: 1.47 us -> 20.6 us  [the longest x1 20.6 us: body(): lax.psum_scatter(unit_term, 'tp', scatter_dimension=1, tiled=True)]
    reduce_sum x7 -> x1, other arithmetic: 12.6 us -> 1.79 us  [body(): mean = jnp.mean(moe_float * moe_float, axis=1, keepdims=True)]
    slice x2 -> x5, local copies, waits for them, and re-layouts: 0.21 us -> 7.98 us  [the longest x2 5.66 us: body(): everyone[:, part_width:2 * part_width]]
    all_to_all x2 -> x1, starting transfers between devices: 12.9 us -> 5.51 us  [body(): lax.all_to_all(expert_rows.reshape(ep_count, capacity, quarter), 'ep', sp...]
  transfers between devices with their start and end apart: 6 -> 5, of which waited for: 2 -> 4; matrix products, arithmetic and copies ran while one was open for 28% -> 23% of each run, Pallas kernels for 0% -> 2%
where the time goes in v1:
time: 217 us
  waiting for transfers between devices  96.9 us (45%)
  matrix products  38.3 us (18%)
  blocking collectives  29.7 us (14%)
  local copies, waits for them, and re-layouts  23.4 us (11%)
  between operations  14 us (6%)
  starting transfers between devices  5.86 us (3%)
  Pallas kernels  4.98 us (2%)
  other arithmetic  3.39 us (2%)
    all_to_all x1, blocking collectives, body(): lax.all_to_all(outgoing.reshape(ep_count, capacity, quarter), 'ep', split...  29.7 us
    all_gather x1, waiting for transfers between devices, body(): everyone = lax.all_gather(shared, 'ep', axis=0, tiled=True)  28 us
    all_gather x1, waiting for transfers between devices, body(): lax.all_gather(arrived, 'tp', axis=0, tiled=True)  26.7 us
    all_to_all x1, waiting for transfers between devices, body(): lax.all_to_all(expert_rows.reshape(ep_count, capacity, quarter), 'ep', sp...  21.5 us
    reduce_scatter x1, waiting for transfers between devices, body(): lax.psum_scatter(unit_term, 'tp', scatter_dimension=1, tiled=True)  20.6 us
    dot_general x1, matrix products, body(): jnp.dot(hidden, expert_down[0], preferred_element_type=f32).astype(bf16)  12 us
    dot_general x3, matrix products, body(): jnp.dot(rows[i], up_w[i], preferred_element_type=f32)  10.7 us
    dot_general x4, matrix products, body(): jnp.dot(rows[i], gate_w[i], preferred_element_type=f32)  9.06 us
  transfers between devices with their start and end apart: 5, of which 4 were waited for; matrix products, arithmetic and copies ran while one was open for 23% of the time, Pallas kernels for 2%

profile of v1, /device:TPU:0, one launch (start us, length us, event | category | flops | bytes accessed | tf_op | source)
XLA Modules:
  0.0 216.5 jit_solution(6685098627439140050)
XLA Ops:
  11.2 2.6 %convolution_convert_fusion.1 = bf16[800,512]{1,0:T(8,128)(2,1)} fusion(s32[384]{0:T(512)S(1)} %get-tuple-element.7, s32[384]{0:T(512)S(1)} %get-tuple-element.6, f32[512]{0:T(512)S(1)} %dynamic_slice.7, f32[384]{0:T(512)S(1)} %add_rsqrt_fusion, bf16[384,2048]{1,0:T(8,128)(2,1)} %param.17, s32[]{:T(128)S(6)} %select_n.43), kind=kOutput, calls=%fused_computation.8 | convolution fusion | flops 316690432 | bytes 1219076 | tf_op jit(solution)/shard_map/dot_general | solution.py:126
  13.8 2.1 reshape.99
  16.0 29.7 %all_to_all.10 = bf16[8,100,512]{2,1,0:T(8,128)(2,1)} all-to-all(bf16[8,100,512]{2,1,0:T(8,128)(2,1)} %reshape.99), channel_id=1, replica_groups=mesh['ep'=8,'tp'=4] {'ep'}, dimensions={0} | all-to-all | bytes 1638400 | tf_op jit(solution)/shard_map/all_to_all | solution.py:127
  45.6 2.1 reshape.100
  48.9 26.7 %all-gather.5.cloned.1.call-done = bf16[3200,512]{1,0:T(8,128)(2,1)} async-done(((bf16[800,512]{1,0:T(8,128)(2,1)}), bf16[3200,512]{1,0:T(8,128)(2,1)}) %all-gather.5.cloned.1.call-update) | async-done | bytes 3276816 | tf_op jit(solution)/shard_map/all_gather | solution.py:151
  75.6 3.8 %fusion.17 = f32[800,768]{1,0:T(8,128)} fusion(bf16[1,2048,768]{2,1,0:T(8,128)(2,1)} %param.22, bf16[3200,512]{1,0:T(8,128)(2,1)} %all-gather.5.cloned.1.call-done), kind=kOutput, calls=%fused_computation.23 | convolution fusion | flops 629145600 | bytes 4063232 | tf_op jit(solution)/shard_map/dot_general | solution.py:155
  79.4 3.4 %fusion.19 = f32[800,768]{1,0:T(8,128)} fusion(bf16[1,2048,768]{2,1,0:T(8,128)(2,1)} %param.22, bf16[3200,512]{1,0:T(8,128)(2,1)S(1)} %copy-done.6), kind=kOutput, calls=%fused_computation.25 | convolution fusion | flops 629145600 | bytes 4063232 | tf_op jit(solution)/shard_map/dot_general | solution.py:155
  82.8 3.6 %fusion.21 = f32[800,768]{1,0:T(8,128)} fusion(bf16[1,2048,768]{2,1,0:T(8,128)(2,1)} %param.22, bf16[3200,512]{1,0:T(8,128)(2,1)S(1)} %copy-done.6), kind=kOutput, calls=%fused_computation.27 | convolution fusion | flops 629145600 | bytes 4063232 | tf_op jit(solution)/shard_map/dot_general | solution.py:155
  86.4 2.3 %fusion.23 = f32[800,768]{1,0:T(8,128)} fusion(bf16[1,2048,768]{2,1,0:T(8,128)(2,1)S(1)} %copy-done.7, bf16[3200,512]{1,0:T(8,128)(2,1)S(1)} %copy-done.6), kind=kOutput, calls=%fused_computation.29 | convolution fusion | flops 629145600 | bytes 4063232 | tf_op jit(solution)/shard_map/dot_general | solution.py:154
  88.6 2.2 %fusion.25 = f32[800,768]{1,0:T(8,128)} fusion(bf16[1,2048,768]{2,1,0:T(8,128)(2,1)S(1)} %copy-done.7, bf16[3200,512]{1,0:T(8,128)(2,1)S(1)} %copy-done.6), kind=kOutput, calls=%fused_computation.31 | convolution fusion | flops 629145600 | bytes 4063232 | tf_op jit(solution)/shard_map/dot_general | solution.py:154
  90.8 2.3 %fusion.27 = f32[800,768]{1,0:T(8,128)} fusion(bf16[1,2048,768]{2,1,0:T(8,128)(2,1)S(1)} %copy-done.7, bf16[3200,512]{1,0:T(8,128)(2,1)S(1)} %copy-done.6), kind=kOutput, calls=%fused_computation.33 | convolution fusion | flops 629145600 | bytes 4063232 | tf_op jit(solution)/shard_map/dot_general | solution.py:154
  93.1 2.3 %fusion.29 = f32[800,768]{1,0:T(8,128)} fusion(bf16[1,2048,768]{2,1,0:T(8,128)(2,1)S(1)} %copy-done.7, bf16[3200,512]{1,0:T(8,128)(2,1)S(1)} %copy-done.6), kind=kOutput, calls=%fused_computation.35 | convolution fusion | flops 629145600 | bytes 4063232 | tf_op jit(solution)/shard_map/dot_general | solution.py:154
  95.4 12.0 %convolution_convert_fusion = bf16[800,2048]{1,0:T(8,128)(2,1)} fusion(bf16[1,768,2048]{2,1,0:T(8,128)(2,1)S(1)} %copy-done, f32[800,768]{1,0:T(8,128)} %fusion.17, f32[800,768]{1,0:T(8,128)} %fusion.21, f32[800,768]{1,0:T(8,128)} %fusion.19, f32[800,768]{1,0:T(8,128)} %fusion.23, f32[800,768]{1,0:T(8,128)} %fusion.25, f32[800,768]{1,0:T(8,128)} %fusion.29, ...), kind=kOutput, calls=%fused_computation | convolution fusion | flops 3154739200 | bytes 25231360 | tf_op jit(solution)/shard_map/dot_general | solution.py:157
  107.8 28.0 %all-gather.3.cloned.1.call-done = bf16[2048,640]{0,1:T(8,128)(2,1)} async-done(((bf16[256,640]{0,1:T(8,128)(2,1)}), bf16[2048,640]{0,1:T(8,128)(2,1)}) %all-gather.3.cloned.1.call-update) | async-done | bytes 2621456 | tf_op jit(solution)/shard_map/all_gather | solution.py:134
  135.8 3.1 %fusion.88 = (bf16[2048,256]{0,1:T(8,128)(2,1)}, bf16[2048,256]{0,1:T(8,128)(2,1)}) fusion(bf16[2048,640]{0,1:T(8,128)(2,1)} %all-gather.3.cloned.1.call-done), kind=kLoop, calls=%fused_computation.111 | loop fusion | bytes 4194304 | tf_op jit(solution)/shard_map/slice | solution.py:143
  139.0 2.3 %copy.21.k_ref = bf16[2048,256]{1,0:T(8,128)(2,1)} copy(bf16[2048,256]{0,1:T(8,128)(2,1)} %get-tuple-element.5) | data formatting | bytes 2097152 | tf_op jit(solution)/shard_map/slice | solution.py:142
  141.3 2.5 %copy.22.v_ref = bf16[2048,256]{1,0:T(8,128)(2,1)} copy(bf16[2048,256]{0,1:T(8,128)(2,1)} %get-tuple-element.4) | data formatting | bytes 2097152 | tf_op jit(solution)/shard_map/slice | solution.py:143
  148.5 5.0 %attention.1 = bf16[256,2048]{1,0:T(8,128)(2,1)S(1)} custom-call(s32[1]{0:T(128)} %bitcast.start_ref, bf16[256,256]{1,0:T(8,128)(2,1)S(1)} %copy-done.5, bf16[2048,256]{1,0:T(8,128)(2,1)S(1)} %copy-done.2, bf16[2048,256]{1,0:T(8,128)(2,1)S(1)} %copy-done.3, f32[256,2]{1,0:T(8,128)S(1)} %copy.23.qt_ref, f32[2,2048]{1,0:T(2,128)S(1)} %fusion.72.kt_ref, ...), custom_call_target="tpu_custom_call" | custom-call | flops 4000000000 | bytes 2097152 | tf_op jit(solution)/shard_map/attention/pallas_call | solution.py:62
  154.5 20.6 %reduce-scatter.5.cloned.1.call-done = bf16[800,512]{1,0:T(8,128)(2,1)} async-done(((bf16[800,2048]{1,0:T(8,128)(2,1)}), bf16[800,512]{1,0:T(8,128)(2,1)}) %reduce-scatter.5.cloned.1.call-update) | async-done | bytes 819216 | tf_op jit(solution)/shard_map/reduce_scatter | solution.py:158
  175.1 2.1 reshape.101
  177.3 5.5 %all-to-all-start.1 = ((bf16[8,100,512]{2,1,0:T(8,128)(2,1)}), bf16[8,100,512]{2,1,0:T(8,128)(2,1)}, u32[]{:S(2)}, u32[]{:S(2)}) async-start(bf16[8,100,512]{2,1,0:T(8,128)(2,1)} %reshape.101), calls=%async_computation.3 | async-start | bytes 1703936 | tf_op jit(solution)/shard_map/all_to_all | solution.py:159
  183.0 21.5 %all-to-all-done.1 = bf16[8,100,512]{2,1,0:T(8,128)(2,1)} async-done(((bf16[8,100,512]{2,1,0:T(8,128)(2,1)}), bf16[8,100,512]{2,1,0:T(8,128)(2,1)}, u32[]{:S(2)}, u32[]{:S(2)}) %all-to-all-start.1) | async-done | bytes 819232 | tf_op jit(solution)/shard_map/all_to_all | solution.py:159
  204.4 2.1 reshape.102
  206.5 1.9 fusion.50
  (55 shorter events, 12.8 us)
Async XLA Ops:
  7.2 88.3 %copy-start = (bf16[1,768,2048]{2,1,0:T(8,128)(2,1)S(1)}, bf16[1,768,2048]{2,1,0:T(8,128)(2,1)}, u32[]{:S(2)}) copy-start(bf16[1,768,2048]{2,1,0:T(8,128)(2,1)} %param.23) | copy-start | bytes 9437188
  7.2 68.4 %all-gather.5.cloned.1.call-start = ((), (), s32[]{:S(2)}) async-start(), calls=%async_computation.6 | async-start | bytes 4096000 | tf_op jit(solution)/shard_map/all_gather | solution.py:151
  15.9 31.9 %copy-start.9 = (bf16[256,256]{1,0:T(8,128)(2,1)S(1)}, bf16[256,256]{1,0:T(8,128)(2,1)}, u32[]{:S(2)}) copy-start(bf16[256,256]{1,0:T(8,128)(2,1)} %param.13) | copy-start | bytes 393220
  16.0 32.0 %copy-start.10 = (bf16[256,256]{1,0:T(8,128)(2,1)S(1)}, bf16[256,256]{1,0:T(8,128)(2,1)}, u32[]{:S(2)}) copy-start(bf16[256,256]{1,0:T(8,128)(2,1)} %param.14) | copy-start | bytes 393220
  16.0 32.1 %copy-start.12 = (f32[256,2]{0,1:T(2,128)S(1)}, f32[256,2]{0,1:T(2,128)}, u32[]{:S(2)}) copy-start(f32[256,2]{0,1:T(2,128)} %param.15) | copy-start | bytes 6148
  47.8 88.1 %all-gather.3.cloned.1.call-start = ((), (), s32[]{:S(2)}) async-start(), calls=%async_computation.4 | async-start | bytes 2949120 | tf_op jit(solution)/shard_map/all_gather | solution.py:134
  48.9 126.3 %reduce-scatter.5.cloned.1.call-start = ((), (), s32[]{:S(2)}) async-start(), calls=%async_computation.7 | async-start | bytes 4096000 | tf_op jit(solution)/shard_map/reduce_scatter | solution.py:158
  75.6 3.8 %copy-start.6 = (bf16[3200,512]{1,0:T(8,128)(2,1)S(1)}, bf16[3200,512]{1,0:T(8,128)(2,1)}, u32[]{:S(2)}) copy-start(bf16[3200,512]{1,0:T(8,128)(2,1)} %all-gather.5.cloned.1.call-done) | copy-start | bytes 9830404
  82.8 3.6 %copy-start.7 = (bf16[1,2048,768]{2,1,0:T(8,128)(2,1)S(1)}, bf16[1,2048,768]{2,1,0:T(8,128)(2,1)}, u32[]{:S(2)}) copy-start(bf16[1,2048,768]{2,1,0:T(8,128)(2,1)} %param.21) | copy-start | bytes 9437188
  107.4 102.6 %reduce-scatter.3.cloned.1.call-start = ((), (), s32[]{:S(2)}) async-start(), calls=%async_computation.5 | async-start | bytes 1310720 | tf_op jit(solution)/shard_map/reduce_scatter | solution.py:149
  139.0 5.6 %copy-start.5 = (bf16[256,256]{1,0:T(8,128)(2,1)S(1)}, bf16[256,256]{1,0:T(8,128)(2,1)}, u32[]{:S(2)}) copy-start(bf16[256,256]{1,0:T(8,128)(2,1)} %q_ref.1) | copy-start | bytes 393220
  144.6 1.4 copy-start.2
  146.0 1.3 copy-start.3
  147.3 1.2 copy-start.4
  153.5 1.0 copy-start.1
  154.5 28.3 %copy-start.11 = (f32[384,2]{0,1:T(2,128)S(1)}, f32[384,2]{0,1:T(2,128)}, u32[]{:S(2)}) copy-start(f32[384,2]{0,1:T(2,128)} %param.20) | copy-start | bytes 9220
  177.3 27.2 %all-to-all-start.1 = ((bf16[8,100,512]{2,1,0:T(8,128)(2,1)}), bf16[8,100,512]{2,1,0:T(8,128)(2,1)}, u32[]{:S(2)}, u32[]{:S(2)}) async-start(bf16[8,100,512]{2,1,0:T(8,128)(2,1)} %reshape.101), calls=%async_computation.3 | async-start | bytes 1703936 | tf_op jit(solution)/shard_map/all_to_all | solution.py:159
  206.5 1.9 copy-start.8
Sparse Core Ops, SparseCore 0:
  47.9 27.6 all-gather.4
  78.2 57.5 all-gather.2
  138.4 36.6 reduce-scatter.4
  178.1 24.7 reduce-scatter.2
